TPU v7x, 32 devices: a whole 2x2x4 slice. The times are simulated.
32 devices in a mesh: sp: 8 (over z, x), tp: 4 (over y, core).
Axes of the slice: x: 2, y: 2, z: 4, core: 2. Of those that a mesh axis runs over, the one named last changes fastest.
Arguments:
- layer_input: bfloat16 [4, 2048, 2048], P(None, ('sp', 'tp')), as said below
- key_weight: bfloat16 [2048, 384], replicated, may hold values from -0.125 to 0.125
- value_weight: bfloat16 [2048, 384], replicated, may hold values from -0.125 to 0.125
- queries: bfloat16 [24, 5, 64], P('sp'), may hold values from -6 to 6
- head_bias: float32 [6, 5], replicated, as said below
Outputs:
- stored: bfloat16 [24, 8, 256, 128], P('sp', None, 'tp')
- first_read: bfloat16 [24, 320], P('sp')
Inputs may be any that keep to these rules, and one draw needn't show every extreme that they name: `layer_input`: entries lie between -12.5 and 12.5. `head_bias`: entries lie between -1 minus the natural logarithm of 2048 and -3.
All inputs are finite; a program needn't handle non-finite values.
Results may differ from a plain program's by a relative error of at most 0.01.
Values may be sent and summed in bfloat16 or wider, within the bound.
A program may use at most 64 MiB of HBM per device.

v0:
```python
import math
import jax
import jax.numpy as jnp
from jax import lax
from jax.sharding import PartitionSpec as P

HD = 64
KVH = 6
GROUP = 5
EPS_NORM = 0.0001


def head_norm(summed):
    squares = jnp.mean(summed * summed, axis=-1, keepdims=True)
    return summed * lax.rsqrt(squares + EPS_NORM)


def shift_table(pair_ids, head_bias):
    heads_range = jnp.arange(KVH, dtype=jnp.int32)
    picker = (pair_ids[:, None] % KVH == heads_range[None, :]).astype(jnp.float32)
    return jnp.dot(picker, head_bias, precision=lax.Precision.HIGHEST)


def per_device(layer_input, key_weight, value_weight, queries, head_bias):
    seq_count, positions, model_width = layer_input.shape
    tokens_flat = layer_input.reshape(seq_count * positions, model_width)
    key_rows = (
        jnp.dot(tokens_flat, key_weight, preferred_element_type=jnp.float32)
        .astype(jnp.bfloat16)
        .reshape(seq_count, positions, KVH, HD)
    )
    value_rows = (
        jnp.dot(tokens_flat, value_weight, preferred_element_type=jnp.float32)
        .astype(jnp.bfloat16)
        .reshape(seq_count, positions, KVH, HD)
    )
    kv_rows = (
        jnp.concatenate([key_rows, value_rows], axis=-1)
        .transpose(0, 2, 1, 3)
        .reshape(seq_count * KVH, 1, positions, 2 * HD)
    )
    stored = lax.all_to_all(kv_rows, "sp", split_axis=0, concat_axis=1, tiled=True)
    score_scale = 1.0 / math.sqrt(HD)
    local_pairs = queries.shape[0]
    pair_ids = lax.axis_index("sp") * local_pairs + jnp.arange(local_pairs, dtype=jnp.int32)
    head_shift = shift_table(pair_ids, head_bias)
    scores = (
        jnp.einsum("pgc,pbtc->pgbt", queries, stored[..., :HD], preferred_element_type=jnp.float32)
        * score_scale
        + head_shift[:, :, None, None]
    )
    keep_log = jax.nn.log_sigmoid(-scores)
    totals = jnp.sum(keep_log, axis=3)
    gathered = lax.all_gather(totals[None], "tp", axis=0, tiled=True)
    later_mask = (jnp.arange(gathered.shape[0], dtype=jnp.int32) > lax.axis_index("tp")).astype(
        jnp.float32
    )
    later_inside = jnp.sum(gathered * later_mask[:, None, None, None], axis=0)
    block_sums = jnp.sum(gathered, axis=0)
    later_blocks = lax.cumsum(block_sums, axis=2, reverse=True) - block_sums
    suffix_log = (
        lax.cumsum(keep_log, axis=3, reverse=True)
        - keep_log
        + (later_inside + later_blocks)[..., None]
    )
    weights = jnp.exp(jax.nn.log_sigmoid(scores) + suffix_log).astype(jnp.bfloat16)
    partial_value = jnp.einsum(
        "pgbt,pbtc->pgc", weights, stored[..., HD:], preferred_element_type=jnp.float32
    )
    summed = lax.psum(partial_value, "tp")
    first_read = head_norm(summed).reshape(local_pairs, GROUP * HD).astype(jnp.bfloat16)
    return (stored, first_read)


def solution(mesh):
    in_specs = (P(None, ("sp", "tp"), None), P(), P(), P("sp", None, None), P())
    out_specs = (P("sp", None, "tp", None), P("sp", None))
    return jax.shard_map(
        per_device, mesh=mesh, in_specs=in_specs, out_specs=out_specs, check_vma=False
    )
```

profile of v0, /device:TPU:0, one launch (start us, length us, event | category | flops | bytes accessed | tf_op | source)
XLA Modules:
  0.0 53.3 jit_solution(13283465844717739790)
XLA Ops:
  0.6 1.4 %copy-done = bf16[2048,384]{1,0:T(8,128)(2,1)S(1)} copy-done((bf16[2048,384]{1,0:T(8,128)(2,1)S(1)}, bf16[2048,384]{1,0:T(8,128)(2,1)}, u32[]{:S(2)}) %copy-start) | copy-done | bytes 1572888
  2.0 2.0 %convolution_convert_fusion.1 = bf16[256,384]{1,0:T(8,128)(2,1)S(1)} fusion(bf16[256,2048]{1,0:T(8,128)(2,1)} %bitcast.33, bf16[2048,384]{1,0:T(8,128)(2,1)S(1)} %copy-done), kind=kOutput, calls=%fused_computation.1 | convolution fusion | flops 402751488 | bytes 2818048 | tf_op jit(solution)/shard_map/dot_general | solution.py:28
  4.1 0.1 copy.26
  4.2 0.2 reshape.69
  4.4 2.1 %convolution_convert_fusion = bf16[256,384]{1,0:T(8,128)(2,1)S(1)} fusion(bf16[256,2048]{1,0:T(8,128)(2,1)S(1)} %bitcast.34, bf16[2048,384]{1,0:T(8,128)(2,1)} %param.7), kind=kOutput, calls=%fused_computation | convolution fusion | flops 402751488 | bytes 2818048 | tf_op jit(solution)/shard_map/dot_general | solution.py:33
  6.6 0.1 copy.27
  6.7 0.2 reshape.70
  6.9 0.6 %maximum_bitcast_fusion = bf16[4,6,64,128]{2,0,3,1:T(4,128)(2,1)S(1)} fusion(bf16[4,64,6,64]{1,0,3,2:T(4,128)(2,1)S(1)} %reshape.70, bf16[4,64,6,64]{1,0,3,2:T(4,128)(2,1)S(1)} %reshape.69), kind=kLoop, calls=%fused_computation.6 | loop fusion | flops 196608 | bytes 786432 | tf_op jit(solution)/shard_map/transpose | solution.py:39
  7.6 1.2 %copy.28 = bf16[4,6,64,128]{3,2,1,0:T(8,128)(2,1)} copy(bf16[4,6,64,128]{2,0,3,1:T(4,128)(2,1)S(1)} %maximum_bitcast_fusion) | data formatting | bytes 786432 | tf_op jit(solution)/shard_map/transpose | solution.py:39
  8.7 7.3 %all-to-all-start = ((bf16[24,1,64,128]{3,2,1,0:T(8,128)(2,1)}), bf16[24,1,64,128]{3,2,1,0:T(8,128)(2,1)S(1)}, u32[]{:S(2)}, u32[]{:S(2)}) async-start(bf16[24,1,64,128]{3,2,1,0:T(8,128)(2,1)} %bitcast.3), calls=%async_computation | async-start | bytes 786432 | tf_op jit(solution)/shard_map/all_to_all | solution.py:42
  16.1 0.2 fusion.15
  16.2 11.5 %all-to-all-done = bf16[24,1,64,128]{3,2,1,0:T(8,128)(2,1)S(1)} async-done(((bf16[24,1,64,128]{3,2,1,0:T(8,128)(2,1)}), bf16[24,1,64,128]{3,2,1,0:T(8,128)(2,1)S(1)}, u32[]{:S(2)}, u32[]{:S(2)}) %all-to-all-start) | async-done | bytes 393248 | tf_op jit(solution)/shard_map/all_to_all | solution.py:42
  27.8 0.5 fusion.9
  28.3 0.1 copy.34
  28.4 5.2 %all-gather = f32[12,5,8]{2,1,0:T(8,128)S(1)} all-gather(f32[3,5,8]{2,1,0:T(8,128)S(1)} %copy.34), channel_id=2, replica_groups=mesh['sp'=8,'tp'=4] {'tp'}, dimensions={0}, use_global_device_ids=true | all-gather | bytes 2400 | tf_op jit(solution)/shard_map/all_gather | solution.py:54
  33.6 0.1 fusion.19
  33.7 0.5 reduce_window_sum.21
  34.2 0.1 copy.35
  34.3 6.4 %reduce_window_sum.20 = f32[3,5,8,64]{3,2,1,0:T(8,128)S(1)} reduce-window(f32[3,5,8,64]{3,2,1,0:T(8,128)S(1)} %copy.32, f32[]{:T(128)} %constant.36.clone.1), window={size=1x1x1x64 pad=0_0x0_0x0_0x0_63}, to_apply=%region_0.1 | reduce-window | flops 483840 | bytes 61444 | tf_op jit(solution)/shard_map/per_device/reduce_window_sum | solution.py:62
  40.7 0.4 convolution_bitcast_fusion
  41.1 11.4 %psum.7 = f32[3,5,64]{2,1,0:T(8,128)S(1)} all-reduce(f32[3,5,64]{2,1,0:T(8,128)S(1)} %convolution_bitcast_fusion), channel_id=1, replica_groups=mesh['sp'=8,'tp'=4] {'tp'}, use_global_device_ids=true, to_apply=%region_5.6 | all-reduce | flops 960 | bytes 7680 | tf_op jit(solution)/shard_map/psum | solution.py:70
  52.5 0.1 multiply_reduce_fusion.1
  52.6 0.1 multiply_convert_fusion
  52.7 0.7 %convert_element_type.28 = bf16[3,320]{1,0:T(4,128)(2,1)} reshape(bf16[3,5,64]{2,1,0:T(8,128)(2,1)S(1)} %multiply_convert_fusion) | data formatting | bytes 3840 | tf_op jit(solution)/shard_map/convert_element_type | solution.py:71
  (16 shorter events, 0.1 us)
Async XLA Ops:
  0.6 1.4 %copy-start = (bf16[2048,384]{1,0:T(8,128)(2,1)S(1)}, bf16[2048,384]{1,0:T(8,128)(2,1)}, u32[]{:S(2)}) copy-start(bf16[2048,384]{1,0:T(8,128)(2,1)} %param.6) | copy-start | bytes 4718596
  2.0 2.4 %copy-start.2 = (bf16[4,64,2048]{2,1,0:T(8,128)(2,1)S(1)}, bf16[4,64,2048]{2,1,0:T(8,128)(2,1)}, u32[]{:S(2)}) copy-start(bf16[4,64,2048]{2,1,0:T(8,128)(2,1)} %param.5) | copy-start | bytes 3145732
  6.9 9.1 %copy-start.4 = (f32[6,5]{1,0:T(8,128)S(1)}, f32[6,5]{1,0:T(8,128)}, u32[]{:S(2)}) copy-start(f32[6,5]{1,0:T(8,128)} %param.9) | copy-start | bytes 364
  7.6 20.2 %copy-start.3 = (bf16[3,5,64]{2,0,1:T(4,128)(2,1)S(1)}, bf16[3,5,64]{2,0,1:T(4,128)(2,1)}, u32[]{:S(2)}) copy-start(bf16[3,5,64]{2,0,1:T(4,128)(2,1)} %param.8) | copy-start | bytes 5764
  8.7 19.0 %all-to-all-start = ((bf16[24,1,64,128]{3,2,1,0:T(8,128)(2,1)}), bf16[24,1,64,128]{3,2,1,0:T(8,128)(2,1)S(1)}, u32[]{:S(2)}, u32[]{:S(2)}) async-start(bf16[24,1,64,128]{3,2,1,0:T(8,128)(2,1)} %bitcast.3), calls=%async_computation | async-start | bytes 786432 | tf_op jit(solution)/shard_map/all_to_all | solution.py:42
  27.7 25.6 %copy-start.1 = (bf16[8,3,1,64,128]{4,3,0,1,2:T(8,128)(2,1)}, bf16[8,3,1,64,128]{4,3,0,1,2:T(8,128)(2,1)S(1)}, u32[]{:S(2)}) copy-start(bf16[8,3,1,64,128]{4,3,0,1,2:T(8,128)(2,1)S(1)} %copy.51) | copy-start | bytes 1179652
where the time goes:
time: 53.7 us; the launch traced here: 53.3 us
  blocking collectives  16.6 us (31%)
  waiting for transfers between devices  11.5 us (21%)
  other arithmetic  7.8 us (15%)
  starting transfers between devices  7.28 us (14%)
  matrix products  5.23 us (10%)
  local copies, waits for them, and re-layouts  4.2 us (8%)
  between operations  0.75 us (1%)
    all_to_all x1, waiting for transfers between devices, per_device(): lax.all_to_all(kv_rows, 'sp', split_axis=0, concat_axis=1, tiled=True)  11.5 us
    psum x1, blocking collectives, per_device(): summed = lax.psum(partial_value, 'tp')  11.4 us
    all_to_all x1, starting transfers between devices, per_device(): lax.all_to_all(kv_rows, 'sp', split_axis=0, concat_axis=1, tiled=True)  7.28 us
    another operation x1, other arithmetic, per_device(): lax.cumsum(keep_log, axis=3, reverse=True) - keep_log  6.41 us
    all_gather x1, blocking collectives, per_device(): gathered = lax.all_gather(totals[None], 'tp', axis=0, tiled=True)  5.21 us
    dot_general x1, matrix products, per_device(): jnp.dot(tokens_flat, value_weight, preferred_element_type=jnp.float32)  2.12 us
    dot_general x1, matrix products, per_device(): jnp.dot(tokens_flat, key_weight, preferred_element_type=jnp.float32)  2.02 us
    unnamed x10, local copies, waits for them, and re-layouts  1.43 us
  transfers between devices with their start and end apart: 1, of which 1 were waited for; matrix products, arithmetic and copies ran while one was open for 0% of the time, Pallas kernels for 0%

commit v1 on v0

--- a/solution.py
+++ b/solution.py
@@ -67,7 +67,7 @@
     partial_value = jnp.einsum(
         "pgbt,pbtc->pgc", weights, stored[..., HD:], preferred_element_type=jnp.float32
     )
-    summed = lax.psum(partial_value, "tp")
+    summed = jnp.sum(lax.all_gather(partial_value, "tp"), axis=0)
     first_read = head_norm(summed).reshape(local_pairs, GROUP * HD).astype(jnp.bfloat16)
     return (stored, first_read)
 

time: 53.7 us -> 47.5 us (0.88)
  blocking collectives: 16.6 us -> 10.4 us
    psum x1 -> x0, blocking collectives: 11.4 us -> none  [per_device(): summed = lax.psum(partial_value, 'tp')]
    all_gather x0 -> x1, blocking collectives: none -> 5.21 us  [per_device(): summed = jnp.sum(lax.all_gather(partial_value, 'tp'), axis=0)]
where the time goes in v1:
time: 47.5 us; the launch traced here: 47.2 us
  waiting for transfers between devices  11.5 us (24%)
  blocking collectives  10.4 us (22%)
  other arithmetic  7.81 us (16%)
  starting transfers between devices  7.28 us (15%)
  matrix products  5.23 us (11%)
  local copies, waits for them, and re-layouts  4.2 us (9%)
  between operations  0.76 us (2%)
    all_to_all x1, waiting for transfers between devices, per_device(): lax.all_to_all(kv_rows, 'sp', split_axis=0, concat_axis=1, tiled=True)  11.5 us
    all_to_all x1, starting transfers between devices, per_device(): lax.all_to_all(kv_rows, 'sp', split_axis=0, concat_axis=1, tiled=True)  7.28 us
    another operation x1, other arithmetic, per_device(): lax.cumsum(keep_log, axis=3, reverse=True) - keep_log  6.41 us
    all_gather x1, blocking collectives, per_device(): summed = jnp.sum(lax.all_gather(partial_value, 'tp'), axis=0)  5.21 us
    all_gather x1, blocking collectives, per_device(): gathered = lax.all_gather(totals[None], 'tp', axis=0, tiled=True)  5.21 us
    dot_general x1, matrix products, per_device(): jnp.dot(tokens_flat, value_weight, preferred_element_type=jnp.float32)  2.12 us
    dot_general x1, matrix products, per_device(): jnp.dot(tokens_flat, key_weight, preferred_element_type=jnp.float32)  2.02 us
    unnamed x10, local copies, waits for them, and re-layouts  1.43 us
  transfers between devices with their start and end apart: 1, of which 1 were waited for; matrix products, arithmetic and copies ran while one was open for 0% of the time, Pallas kernels for 0%

profile of v1, /device:TPU:0, one launch (start us, length us, event | category | flops | bytes accessed | tf_op | source)
XLA Modules:
  0.0 47.2 jit_solution(7443517885763475087)
XLA Ops:
  0.6 1.4 %copy-done = bf16[2048,384]{1,0:T(8,128)(2,1)S(1)} copy-done((bf16[2048,384]{1,0:T(8,128)(2,1)S(1)}, bf16[2048,384]{1,0:T(8,128)(2,1)}, u32[]{:S(2)}) %copy-start) | copy-done | bytes 1572888
  2.0 2.0 %convolution_convert_fusion.1 = bf16[256,384]{1,0:T(8,128)(2,1)S(1)} fusion(bf16[256,2048]{1,0:T(8,128)(2,1)} %bitcast.35, bf16[2048,384]{1,0:T(8,128)(2,1)S(1)} %copy-done), kind=kOutput, calls=%fused_computation.1 | convolution fusion | flops 402751488 | bytes 2818048 | tf_op jit(solution)/shard_map/dot_general | solution.py:28
  4.1 0.1 copy.26
  4.2 0.2 reshape.72
  4.4 2.1 %convolution_convert_fusion = bf16[256,384]{1,0:T(8,128)(2,1)S(1)} fusion(bf16[256,2048]{1,0:T(8,128)(2,1)S(1)} %bitcast.36, bf16[2048,384]{1,0:T(8,128)(2,1)} %param.7), kind=kOutput, calls=%fused_computation | convolution fusion | flops 402751488 | bytes 2818048 | tf_op jit(solution)/shard_map/dot_general | solution.py:33
  6.6 0.1 copy.27
  6.7 0.2 reshape.73
  6.9 0.6 %maximum_bitcast_fusion = bf16[4,6,64,128]{2,0,3,1:T(4,128)(2,1)S(1)} fusion(bf16[4,64,6,64]{1,0,3,2:T(4,128)(2,1)S(1)} %reshape.73, bf16[4,64,6,64]{1,0,3,2:T(4,128)(2,1)S(1)} %reshape.72), kind=kLoop, calls=%fused_computation.6 | loop fusion | flops 196608 | bytes 786432 | tf_op jit(solution)/shard_map/transpose | solution.py:39
  7.6 1.2 %copy.28 = bf16[4,6,64,128]{3,2,1,0:T(8,128)(2,1)} copy(bf16[4,6,64,128]{2,0,3,1:T(4,128)(2,1)S(1)} %maximum_bitcast_fusion) | data formatting | bytes 786432 | tf_op jit(solution)/shard_map/transpose | solution.py:39
  8.7 7.3 %all-to-all-start = ((bf16[24,1,64,128]{3,2,1,0:T(8,128)(2,1)}), bf16[24,1,64,128]{3,2,1,0:T(8,128)(2,1)S(1)}, u32[]{:S(2)}, u32[]{:S(2)}) async-start(bf16[24,1,64,128]{3,2,1,0:T(8,128)(2,1)} %bitcast.3), calls=%async_computation | async-start | bytes 786432 | tf_op jit(solution)/shard_map/all_to_all | solution.py:42
  16.1 0.2 fusion.15
  16.2 11.5 %all-to-all-done = bf16[24,1,64,128]{3,2,1,0:T(8,128)(2,1)S(1)} async-done(((bf16[24,1,64,128]{3,2,1,0:T(8,128)(2,1)}), bf16[24,1,64,128]{3,2,1,0:T(8,128)(2,1)S(1)}, u32[]{:S(2)}, u32[]{:S(2)}) %all-to-all-start) | async-done | bytes 393248 | tf_op jit(solution)/shard_map/all_to_all | solution.py:42
  27.8 0.5 %fusion.9 = (f32[3,5,8]{1,2,0:T(8,128)S(1)}, f32[3,5,8,64]{3,1,2,0:T(8,128)S(1)}, f32[3,5,8,64]{3,1,2,0:T(8,128)S(1)}) fusion(f32[3,5]{1,0:T(4,128)S(1)} %fusion.15, bf16[3,5,64,1]{2,0,1,3:T(4,128)(2,1)S(1)} %bitcast.37, bf16[3,8,64,128]{3,2,1,0:T(8,128)(2,1)S(1)} %bitcast.30), kind=kOutput, calls=%fused_computation.18 | convolution fusion | flops 1059720 | bytes 457116 | tf_op jit(solution)/shard_map/pgc,pbtc->pgbt/dot_general | solution.py:48
  28.3 0.1 copy.34
  28.4 5.2 %all-gather = f32[12,5,8]{2,1,0:T(8,128)S(1)} all-gather(f32[3,5,8]{2,1,0:T(8,128)S(1)} %copy.34), channel_id=2, replica_groups=mesh['sp'=8,'tp'=4] {'tp'}, dimensions={0}, use_global_device_ids=true | all-gather | bytes 2400 | tf_op jit(solution)/shard_map/all_gather | solution.py:54
  33.6 0.1 fusion.19
  33.7 0.5 %reduce_window_sum.21 = f32[3,5,8]{2,1,0:T(8,128)S(1)} reduce-window(f32[3,5,8]{2,1,0:T(8,128)S(1)} %get-tuple-element.2, f32[]{:T(128)} %constant.36.clone.1), window={size=1x1x8 pad=0_0x0_0x0_7}, to_apply=%region_4.5 | reduce-window | flops 840 | bytes 964 | tf_op jit(solution)/shard_map/per_device/reduce_window_sum | solution.py:60
  34.2 0.1 copy.35
  34.3 6.4 %reduce_window_sum.20 = f32[3,5,8,64]{3,2,1,0:T(8,128)S(1)} reduce-window(f32[3,5,8,64]{3,2,1,0:T(8,128)S(1)} %copy.32, f32[]{:T(128)} %constant.36.clone.1), window={size=1x1x1x64 pad=0_0x0_0x0_0x0_63}, to_apply=%region_0.1 | reduce-window | flops 483840 | bytes 61444 | tf_op jit(solution)/shard_map/per_device/reduce_window_sum | solution.py:62
  40.7 0.4 convolution_bitcast_fusion
  41.1 5.2 %all-gather.1 = f32[12,5,64]{2,1,0:T(8,128)S(1)} all-gather(f32[3,5,64]{2,1,0:T(8,128)S(1)} %convolution_bitcast_fusion), channel_id=3, replica_groups=mesh['sp'=8,'tp'=4] {'tp'}, dimensions={0}, use_global_device_ids=true | all-gather | bytes 19200 | tf_op jit(solution)/shard_map/all_gather | solution.py:70
  46.3 0.1 multiply_reduce_fusion.1
  46.4 0.1 multiply_convert_fusion
  46.5 0.7 %convert_element_type.28 = bf16[3,320]{1,0:T(4,128)(2,1)} reshape(bf16[3,5,64]{2,1,0:T(8,128)(2,1)S(1)} %multiply_convert_fusion) | data formatting | bytes 3840 | tf_op jit(solution)/shard_map/convert_element_type | solution.py:71
  (17 shorter events, 0.1 us)
Async XLA Ops:
  0.6 1.4 %copy-start = (bf16[2048,384]{1,0:T(8,128)(2,1)S(1)}, bf16[2048,384]{1,0:T(8,128)(2,1)}, u32[]{:S(2)}) copy-start(bf16[2048,384]{1,0:T(8,128)(2,1)} %param.6) | copy-start | bytes 4718596
  2.0 2.4 %copy-start.2 = (bf16[4,64,2048]{2,1,0:T(8,128)(2,1)S(1)}, bf16[4,64,2048]{2,1,0:T(8,128)(2,1)}, u32[]{:S(2)}) copy-start(bf16[4,64,2048]{2,1,0:T(8,128)(2,1)} %param.5) | copy-start | bytes 3145732
  6.9 9.1 %copy-start.4 = (f32[6,5]{1,0:T(8,128)S(1)}, f32[6,5]{1,0:T(8,128)}, u32[]{:S(2)}) copy-start(f32[6,5]{1,0:T(8,128)} %param.9) | copy-start | bytes 364
  7.6 20.2 %copy-start.3 = (bf16[3,5,64]{2,0,1:T(4,128)(2,1)S(1)}, bf16[3,5,64]{2,0,1:T(4,128)(2,1)}, u32[]{:S(2)}) copy-start(bf16[3,5,64]{2,0,1:T(4,128)(2,1)} %param.8) | copy-start | bytes 5764
  8.7 19.0 %all-to-all-start = ((bf16[24,1,64,128]{3,2,1,0:T(8,128)(2,1)}), bf16[24,1,64,128]{3,2,1,0:T(8,128)(2,1)S(1)}, u32[]{:S(2)}, u32[]{:S(2)}) async-start(bf16[24,1,64,128]{3,2,1,0:T(8,128)(2,1)} %bitcast.3), calls=%async_computation | async-start | bytes 786432 | tf_op jit(solution)/shard_map/all_to_all | solution.py:42
  27.7 19.4 %copy-start.1 = (bf16[8,3,1,64,128]{4,3,0,1,2:T(8,128)(2,1)}, bf16[8,3,1,64,128]{4,3,0,1,2:T(8,128)(2,1)S(1)}, u32[]{:S(2)}) copy-start(bf16[8,3,1,64,128]{4,3,0,1,2:T(8,128)(2,1)S(1)} %copy.51) | copy-start | bytes 1179652
